TPU v7x, 128 devices: a whole 4x4x4 slice. The times are simulated.
128 devices in a mesh: rep: 2 (over z_hi), fs: 32 (over z_lo, y, x), tp: 2 (over core).
Axes of the slice: x: 4, y: 4, z: 4 (z_hi: 2, z_lo: 2; z = z_hi * 2 + z_lo), core: 2. Of those that a mesh axis runs over, the one named last changes fastest.
Arguments:
- residual: bfloat16 [32768, 2048], P(('rep', 'fs', 'tp')), may hold values from -6 to 6
- mixer_gain: float32 [2048], replicated, may hold values from 0.1 to 1.9
- gating_proj: bfloat16 [2048, 2048], P('fs', 'tp'), may hold values from -0.125 to 0.125
- spatial_proj: bfloat16 [2048, 2048], P('fs', 'tp'), as said below
- spatial_gain: float32 [2048], replicated, may hold values from 0.1 to 1.9
- spatial_bias: float32 [2048], replicated, may hold values from -3 to 3
- spatial_mix: bfloat16 [32, 128, 128], replicated, may hold values from -0.5 to 0.5
- spatial_offset: float32 [32, 128], replicated, may hold values from 0.5 to 1.5
- mixer_out: bfloat16 [2048, 2048], P('tp', 'fs'), may hold values from -0.125 to 0.125
- channel_gain: float32 [2048], replicated, may hold values from 0.1 to 1.9
- gate_proj: bfloat16 [2048, 2816], P('fs', 'tp'), may hold values from -0.125 to 0.125
- up_proj: bfloat16 [2048, 2816], P('fs', 'tp'), may hold values from -0.125 to 0.125
- conv_taps: float32 [3, 2816], replicated, may hold values from -3.5 to 3.5
- down_proj: bfloat16 [2816, 2048], P('tp', 'fs'), may hold values from -0.109375 to 0.109375
Outputs:
- layer_out: bfloat16 [32768, 2048], P(('rep', 'fs', 'tp'))
Inputs may be any that keep to these rules, and one draw needn't show every extreme that they name: `spatial_proj`: entries are bounded in magnitude by 56 / sqrt(2048).
All inputs are finite; a program needn't handle non-finite values.
Results may differ from a plain program's by a relative error of at most 0.015.
Values may be sent and summed in bfloat16 or wider, within the bound.
No kernel may reach another device: no remote copies, remote signals or barrier semaphores. Data moves between devices by JAX's collectives and lax.ppermute only.
A program may use at most 128 MiB of HBM per device.

v0:
```python
import jax
import jax.numpy as jnp
from jax import lax
from jax.sharding import Mesh
from jax.sharding import PartitionSpec as P

HEAD = 64
GROUP = 2048
BLOCK = 128
SEGMENT = 64
KCONV = 3
SEQ_LEN = 256
FS = ("fs_0", "fs_1", "fs_2")
REP_FS_TP = ("rep", "fs_0", "fs_1", "fs_2", "tp")


def in_order(pieces, dim):
    pieces = jnp.moveaxis(pieces, 0, dim)
    lengths = pieces.shape
    return pieces.reshape(*lengths[:dim], lengths[dim] * lengths[dim + 1], *lengths[dim + 2 :])


def copy_for_each(value, axis):
    devices = lax.axis_size(axis)
    return lax.all_to_all(
        jnp.broadcast_to(value[None], (devices, *value.shape)), axis, 0, 0, tiled=True
    )


def gathered_copies(value, axis, dim):
    return in_order(copy_for_each(value, axis), dim)


def side_by_side(arrays, axis, dim, along):
    widths = [a.shape[along] for a in arrays]
    both = jnp.concatenate(arrays, axis=along)
    out = lax.all_gather(both, axis, axis=dim, tiled=True)
    return tuple(jnp.split(out, [sum(widths[:k]) for k in range(1, len(widths))], axis=along))


def of_everyone(value, axis):
    return copy_for_each(value, axis).sum(axis=0)


def in_one(arrays, axis):
    ends = [0]
    for a in arrays:
        ends.append(ends[-1] + a.size)
    running = of_everyone(jnp.concatenate([a.ravel() for a in arrays]), axis)
    return tuple((running[b:e].reshape(a.shape) for a, b, e in zip(arrays, ends, ends[1:])))


def stacked_from(value, axes, order):
    pieces = value[None]
    for k in order:
        pieces = lax.all_gather(pieces, axes[k], axis=0, tiled=True)
    block = [lax.axis_size(axes[k]) for k in reversed(order)]
    pieces = pieces.reshape(*block, *value.shape)
    turned = sorted(range(len(order)), key=lambda place: order[len(order) - 1 - place])
    return pieces.transpose(*turned, *range(len(order), pieces.ndim)).reshape(-1, *value.shape)


def gather_axes(value, axes, order, dim):
    return in_order(stacked_from(value, axes, order), dim)


def cut_along(value, dim, devices):
    before, after = (value.shape[:dim], value.shape[dim + 1 :])
    return jnp.moveaxis(value.reshape(*before, devices, -1, *after), dim, 0)


def sum_at_owner(value, axis, dim):
    pieces = cut_along(value, dim, lax.axis_size(axis))
    arrived = lax.all_to_all(pieces, axis, split_axis=0, concat_axis=0, tiled=True)
    return arrived.astype(jnp.float32).sum(axis=0)


def round_trip(value):
    return lax.optimization_barrier(value.astype(jnp.bfloat16)).astype(jnp.float32)


def rms_normed(value, gain):
    wide = value.astype(jnp.float32)
    scale = lax.rsqrt(jnp.mean(wide * wide, axis=-1, keepdims=True) + 1e-06)
    return (wide * scale * gain).astype(jnp.bfloat16)


def fold_pair(normed, pieces):
    first = jnp.dot(normed, pieces[0], preferred_element_type=jnp.float32)
    second = jnp.dot(normed, pieces[1], preferred_element_type=jnp.float32)
    return (first, second)


def on_device(
    residual,
    mixer_gain,
    gating_proj,
    spatial_proj,
    spatial_gain,
    spatial_bias,
    spatial_mix,
    spatial_offset,
    mixer_out,
    channel_gain,
    gate_proj,
    up_proj,
    conv_taps,
    down_proj,
):
    position = lax.axis_index("tp")
    rows = gathered_copies(residual, "tp", 0)
    group_rows = rows.shape[0]
    normed = rms_normed(rows, mixer_gain)
    width = gating_proj.shape[1]
    gating, spatial = fold_pair(normed, side_by_side((gating_proj, spatial_proj), FS, 0, 1))
    act_u = jax.nn.gelu(round_trip(gating))
    act_v = jax.nn.gelu(round_trip(spatial))
    total, squares = in_one((jnp.sum(act_v, axis=-1), jnp.sum(act_v * act_v, axis=-1)), "tp")
    mean = (total / GROUP)[:, None]
    var = (squares / GROUP)[:, None] - mean * mean
    gain_here = lax.dynamic_slice_in_dim(spatial_gain, position * width, width)
    bias_here = lax.dynamic_slice_in_dim(spatial_bias, position * width, width)
    vnorm = ((act_v - mean) * lax.rsqrt(var + 1e-05) * gain_here + bias_here).astype(jnp.bfloat16)
    heads_here = width // HEAD
    mix_here = lax.dynamic_slice_in_dim(spatial_mix, position * heads_here, heads_here, 0)
    offset_here = lax.dynamic_slice_in_dim(spatial_offset, position * heads_here, heads_here, 0)
    place = jnp.arange(BLOCK) // SEGMENT
    allowed = place[None, :] <= place[:, None]
    weights = jnp.where(allowed[None], mix_here, jnp.zeros_like(mix_here))
    blocks = vnorm.reshape(group_rows // BLOCK, BLOCK, heads_here, HEAD)
    mixed = jnp.einsum("hij,njhd->nihd", weights, blocks, preferred_element_type=jnp.float32)
    mixed = mixed + offset_here.T[None, :, :, None]
    gated = (act_u * mixed.reshape(group_rows, width)).astype(jnp.bfloat16)
    out_whole = gather_axes(mixer_out, FS, (0, 1, 2), 1)
    part = gated
    mixer_part = sum_at_owner(
        jnp.dot(part, out_whole, preferred_element_type=jnp.float32).astype(jnp.bfloat16), "tp", 0
    )
    middle = (residual.astype(jnp.float32) + mixer_part).astype(jnp.bfloat16)
    rows2 = gathered_copies(middle, "tp", 0)
    normed2 = rms_normed(rows2, channel_gain)
    units = gate_proj.shape[1]
    gate_whole, up_whole = side_by_side((gate_proj, up_proj), FS, 0, 1)
    gate = jnp.dot(normed2, gate_whole, preferred_element_type=jnp.float32)
    up = jnp.dot(normed2, up_whole, preferred_element_type=jnp.float32)
    gate = round_trip(gate)
    up = round_trip(up)
    taps_here = lax.dynamic_slice_in_dim(conv_taps, position * units, units, 1)
    offset = jnp.arange(group_rows) % SEQ_LEN
    conv = taps_here[KCONV - 1] * gate
    for lag in range(1, KCONV):
        shifted = jnp.concatenate([jnp.zeros((lag, units), jnp.float32), gate[:-lag]], axis=0)
        shifted = jnp.where((offset >= lag)[:, None], shifted, 0.0)
        conv = conv + taps_here[KCONV - 1 - lag] * shifted
    hidden = (jax.nn.silu(conv) * up).astype(jnp.bfloat16)
    down_whole = lax.all_gather(down_proj, FS, axis=1, tiled=True)
    part = hidden
    channel_part = sum_at_owner(
        jnp.dot(part, down_whole, preferred_element_type=jnp.float32).astype(jnp.bfloat16), "tp", 0
    )
    return (middle.astype(jnp.float32) + channel_part).astype(jnp.bfloat16)


def solution(mesh):
    split = Mesh(
        mesh.devices.reshape(mesh.shape["rep"], 2, 4, 4, mesh.shape["tp"]),
        ("rep", "fs_0", "fs_1", "fs_2", "tp"),
    )
    placed = (
        P(REP_FS_TP, None),
        P(),
        P(FS, "tp"),
        P(FS, "tp"),
        P(),
        P(),
        P(),
        P(),
        P("tp", FS),
        P(),
        P(FS, "tp"),
        P(FS, "tp"),
        P(),
        P("tp", FS),
    )
    return jax.shard_map(
        on_device, mesh=split, in_specs=placed, out_specs=P(REP_FS_TP, None), check_vma=False
    )
```

profile of v0, /device:TPU:1, one launch (start us, length us, event | category | flops | bytes accessed | tf_op | source)
XLA Modules:
  0.0 617.4 jit_solution(9370628572742280357)
XLA Ops:
  6.6 6.7 %all-gather = bf16[2048,64]{0,1:T(8,128)(2,1)S(1)} all-gather(bf16[1024,64]{0,1:T(8,128)(2,1)} %param.22), channel_id=2, replica_groups=mesh['rep'=2,'fs_0'=2,'fs_1'=4,'fs_2'=4,'tp'=2] {'fs_0'}, dimensions={0}, use_global_device_ids=true | all-gather | bytes 393216 | tf_op jit(solution)/shard_map/all_gather | solution.py:56
  13.3 0.7 copy.73
  14.1 0.0 all-gather.11.cloned.1.call-start
  14.1 24.9 %all-gather.9.cloned.1.call-done = bf16[8,1024,64]{1,2,0:T(8,128)(2,1)} async-done(((bf16[2,1024,64]{1,2,0:T(8,128)(2,1)}), bf16[8,1024,64]{1,2,0:T(8,128)(2,1)}) %all-gather.9.cloned.1.call-update) | async-done | bytes 1048592 | tf_op jit(solution)/shard_map/all_gather | solution.py:56
  39.1 0.7 pad_maximum_fusion.1
  39.8 0.0 all-gather.13.cloned.1.call-start
  39.9 0.8 pad_maximum_fusion
  40.7 0.5 all-gather.15.cloned.1.call-update
  41.3 1.6 broadcast_in_dim.32
  42.9 6.5 %all-to-all-start = ((bf16[2,256,2048]{2,1,0:T(8,128)(2,1)}), bf16[2,256,2048]{2,1,0:T(8,128)(2,1)S(1)}, u32[]{:S(2)}, u32[]{:S(2)}) async-start(bf16[2,256,2048]{2,1,0:T(8,128)(2,1)} %broadcast_in_dim.32), calls=%async_computation | async-start | bytes 4194304 | tf_op jit(solution)/shard_map/all_to_all | solution.py:25
  49.4 2.5 all-to-all-done
  51.9 0.5 multiply_reduce_fusion.1
  52.4 1.6 dynamic-slice_reduce_fusion.2
  54.0 0.6 fusion.61
  54.6 0.1 broadcast_compare_fusion
  54.7 1.9 fusion.11
  56.5 34.6 %all-gather.11.cloned.1.call-done = bf16[32,1024,64]{1,2,0:T(8,128)(2,1)} async-done(((bf16[8,1024,64]{1,2,0:T(8,128)(2,1)}), bf16[32,1024,64]{1,2,0:T(8,128)(2,1)}) %all-gather.11.cloned.1.call-update) | async-done | bytes 4194320 | tf_op jit(solution)/shard_map/all_gather | solution.py:56
  91.1 4.9 copy.56
  96.0 143.2 %all-gather.7.cloned.1.call-done = bf16[2048,2048]{1,0:T(8,128)(2,1)} async-done(((bf16[64,2048]{1,0:T(8,128)(2,1)}), bf16[2048,2048]{1,0:T(8,128)(2,1)}) %all-gather.7.cloned.1.call-update) | async-done | bytes 8388624 | tf_op jit(solution)/shard_map/all_gather | solution.py:37
  239.2 5.1 fusion.37
  244.3 1.0 fusion.52
  245.3 24.3 %all_to_all.26 = f32[2,1,1024]{2,1,0:T(1,128)S(1)} all-to-all(f32[2,1,1024]{2,1,0:T(1,128)S(1)} %broadcast_in_dim.33), channel_id=1, replica_groups=mesh['rep'=2,'fs_0'=2,'fs_1'=4,'fs_2'=4,'tp'=2] {'tp'}, dimensions={0} | all-to-all | bytes 16384 | tf_op jit(solution)/shard_map/all_to_all | solution.py:25
  269.7 1.0 add_convert_fusion.2
  270.7 2.3 reshape.157
  273.1 2.7 bitcast_add_fusion
  275.8 3.0 copy.60
  278.8 3.5 reshape.158
  282.3 5.4 fusion.34
  287.7 2.7 convolution_convert_fusion
  290.4 5.3 all_to_all.27
  295.8 0.4 convert_reduce_fusion.1
  296.2 0.3 add_convert_fusion.1
  296.6 0.3 broadcast_in_dim.37
  296.8 5.5 all_to_all.28
  302.3 0.5 multiply_reduce_fusion
  302.9 0.2 copy-done.10
  303.0 1.9 fusion.9
  304.9 109.0 %all-gather.13.cloned.1.call-done = bf16[2048,2816]{1,0:T(8,128)(2,1)} async-done(((bf16[64,2816]{1,0:T(8,128)(2,1)}), bf16[2048,2816]{1,0:T(8,128)(2,1)}) %all-gather.13.cloned.1.call-update) | async-done | bytes 11534352 | tf_op jit(solution)/shard_map/all_gather | solution.py:37
  413.9 6.8 %fusion.12 = bf16[512,1408]{1,0:T(8,128)(2,1)S(1)} fusion(bf16[512,2048]{1,0:T(8,128)(2,1)} %fusion.9, bf16[2048,2816]{1,0:T(8,128)(2,1)} %all-gather.13.cloned.1.call-done), kind=kOutput, calls=%fused_computation.27 | convolution fusion | flops 2953510912 | bytes 9306112 | tf_op jit(solution)/shard_map/dot_general | solution.py:144
  420.7 1.7 slice.28
  422.4 1.9 slice.29
  424.3 1.2 copy-done.4
  425.5 4.5 fusion.15
  430.0 144.2 %all-gather.15.cloned.1.call-done = bf16[1408,2048]{0,1:T(8,128)(2,1)} async-done(((bf16[1408,64]{0,1:T(8,128)(2,1)}), bf16[1408,2048]{0,1:T(8,128)(2,1)}) %all-gather.15.cloned.1.call-update) | async-done | bytes 5767184 | tf_op jit(solution)/shard_map/all_gather | solution.py:156
  574.2 9.8 %convolution_convert_fusion.1 = bf16[512,2048]{1,0:T(8,128)(2,1)S(1)} fusion(bf16[1408,2048]{0,1:T(8,128)(2,1)} %all-gather.15.cloned.1.call-done, bf16[512,1408]{1,0:T(8,128)(2,1)} %fusion.15, f32[510,1408]{1,0:T(8,128)} %slice.29, f32[511,1408]{1,0:T(8,128)} %slice.28, f32[1408]{0:T(1024)S(1)} %copy-done.13, f32[1408]{0:T(1024)S(1)} %copy-done.12, ...), kind=kOutput, calls=%fused_computation.29 | convolution fusion | flops 2964652032 | bytes 16516096 | tf_op jit(solution)/shard_map/dot_general | solution.py:159
  584.0 25.1 %all_to_all.29 = bf16[2,256,2048]{2,1,0:T(8,128)(2,1)S(1)} all-to-all(bf16[2,256,2048]{2,1,0:T(8,128)(2,1)S(1)} %bitcast.51), channel_id=1, replica_groups=mesh['rep'=2,'fs_0'=2,'fs_1'=4,'fs_2'=4,'tp'=2] {'tp'}, dimensions={0} | all-to-all | bytes 4194304 | tf_op jit(solution)/shard_map/all_to_all | solution.py:74
  609.1 0.4 convert_reduce_fusion
  609.6 1.3 add_convert_fusion
  (58 shorter events, 0.3 us)
Async XLA Ops:
  6.5 48.0 %copy-start = (f32[32,128]{1,0:T(8,128)S(1)}, f32[32,128]{1,0:T(8,128)}, u32[]{:S(2)}) copy-start(f32[32,128]{1,0:T(8,128)} %param.21) | copy-start | bytes 49156
  6.5 32.5 %copy-start.8 = (bf16[64,1024]{1,0:T(8,128)(2,1)S(1)}, bf16[64,1024]{1,0:T(8,128)(2,1)}, u32[]{:S(2)}) copy-start(bf16[64,1024]{1,0:T(8,128)(2,1)} %param.16) | copy-start | bytes 393220
  6.5 32.5 %copy-start.7 = (bf16[64,1024]{1,0:T(8,128)(2,1)S(1)}, bf16[64,1024]{1,0:T(8,128)(2,1)}, u32[]{:S(2)}) copy-start(bf16[64,1024]{1,0:T(8,128)(2,1)} %param.17) | copy-start | bytes 393220
  6.5 33.3 %copy-start.6 = (bf16[64,1408]{1,0:T(8,128)(2,1)S(1)}, bf16[64,1408]{1,0:T(8,128)(2,1)}, u32[]{:S(2)}) copy-start(bf16[64,1408]{1,0:T(8,128)(2,1)} %param.24) | copy-start | bytes 540676
  6.5 33.3 %copy-start.5 = (bf16[64,1408]{1,0:T(8,128)(2,1)S(1)}, bf16[64,1408]{1,0:T(8,128)(2,1)}, u32[]{:S(2)}) copy-start(bf16[64,1408]{1,0:T(8,128)(2,1)} %param.25) | copy-start | bytes 540676
  6.5 34.7 %copy-start.3 = (bf16[256,2048]{1,0:T(8,128)(2,1)S(1)}, bf16[256,2048]{1,0:T(8,128)(2,1)}, u32[]{:S(2)}) copy-start(bf16[256,2048]{1,0:T(8,128)(2,1)} %param.14) | copy-start | bytes 3145732
  6.6 32.4 %all-gather.9.cloned.1.call-start = ((), (), s32[]{:S(2)}) async-start(), calls=%async_computation.6 | async-start | bytes 1310720 | tf_op jit(solution)/shard_map/all_gather | solution.py:56
  14.1 77.0 %all-gather.11.cloned.1.call-start = ((), (), s32[]{:S(2)}) async-start(), calls=%async_computation.7 | async-start | bytes 5242880 | tf_op jit(solution)/shard_map/all_gather | solution.py:56
  39.0 200.2 %all-gather.7.cloned.1.call-start = ((), (), s32[]{:S(2)}) async-start(), calls=%async_computation.5 | async-start | bytes 8650752 | tf_op jit(solution)/shard_map/all_gather | solution.py:37
  39.8 374.0 %all-gather.13.cloned.1.call-start = ((), (), s32[]{:S(2)}) async-start(), calls=%async_computation.8 | async-start | bytes 11894784 | tf_op jit(solution)/shard_map/all_gather | solution.py:37
  40.7 533.5 %all-gather.15.cloned.1.call-start = ((), (), s32[]{:S(2)}) async-start(), calls=%async_computation.9 | async-start | bytes 5947392 | tf_op jit(solution)/shard_map/all_gather | solution.py:156
  42.9 9.0 %all-to-all-start = ((bf16[2,256,2048]{2,1,0:T(8,128)(2,1)}), bf16[2,256,2048]{2,1,0:T(8,128)(2,1)S(1)}, u32[]{:S(2)}, u32[]{:S(2)}) async-start(bf16[2,256,2048]{2,1,0:T(8,128)(2,1)} %broadcast_in_dim.32), calls=%async_computation | async-start | bytes 4194304 | tf_op jit(solution)/shard_map/all_to_all | solution.py:25
  49.4 5.3 copy-start.9
  96.0 173.8 %dynamic-slice-start = ((f32[2048]{0:T(1024)}, s32[]{:T(128)}), f32[1024]{0:T(1024)S(1)}, s32[]{:S(2)}) async-start(f32[2048]{0:T(1024)} %param.18, s32[]{:T(128)} %select_n.51), calls=%async_computation.10 | async-start | bytes 8704 | tf_op jit(solution)/shard_map/dynamic_slice | solution.py:121
  96.0 173.8 %dynamic-slice-start.1 = ((f32[2048]{0:T(1024)}, s32[]{:T(128)}), f32[1024]{0:T(1024)S(1)}, s32[]{:S(2)}) async-start(f32[2048]{0:T(1024)} %param.19, s32[]{:T(128)} %select_n.51), calls=%async_computation.11 | async-start | bytes 8704 | tf_op jit(solution)/shard_map/dynamic_slice | solution.py:122
  282.3 5.4 copy-start.2
  302.3 0.7 copy-start.10
  413.9 10.4 %slice-start = ((s8[11534336]{0:T(1024)(128)(4,1)}), s8[4194304]{0:T(1024)(128)(4,1)S(1)}, s32[]{:S(2)}) async-start(s8[11534336]{0:T(1024)(128)(4,1)} %bitcast.57), calls=%async_computation.12 | async-start | bytes 8388608
  413.9 10.4 %slice-start.1 = ((s8[11534336]{0:T(1024)(128)(4,1)}), s8[4194304]{0:T(1024)(128)(4,1)S(1)}, s32[]{:S(2)}) async-start(s8[11534336]{0:T(1024)(128)(4,1)} %bitcast.57), calls=%async_computation.13 | async-start | bytes 8388608
  420.7 3.6 slice-start.2
  422.4 3.1 copy-start.4
  425.5 148.7 %copy-start.11 = (f32[1408]{0:T(1024)S(1)}, f32[1408]{0:T(1024)}, u32[]{:S(2)}) copy-start(f32[1408]{0:T(1024)} %get-tuple-element.7) | copy-start | bytes 16900
  425.5 148.7 %copy-start.12 = (f32[1408]{0:T(1024)S(1)}, f32[1408]{0:T(1024)}, u32[]{:S(2)}) copy-start(f32[1408]{0:T(1024)} %get-tuple-element.8) | copy-start | bytes 16900
  425.5 148.7 %copy-start.13 = (f32[1408]{0:T(1024)S(1)}, f32[1408]{0:T(1024)}, u32[]{:S(2)}) copy-start(f32[1408]{0:T(1024)} %get-tuple-element.9) | copy-start | bytes 16900
  425.5 148.7 %copy-start.14 = (pred[512]{0:T(512)(128)(4,1)S(1)}, pred[512]{0:T(512)(128)(4,1)}, u32[]{:S(2)}) copy-start(pred[512]{0:T(512)(128)(4,1)} %get-tuple-element.12) | copy-start | bytes 1540
  425.5 148.7 %copy-start.15 = (pred[512]{0:T(512)(128)(4,1)S(1)}, pred[512]{0:T(512)(128)(4,1)}, u32[]{:S(2)}) copy-start(pred[512]{0:T(512)(128)(4,1)} %get-tuple-element.13) | copy-start | bytes 1540
  609.1 1.8 copy-start.1
Sparse Core Ops, SparseCore 0:
  14.2 24.7 all-gather.8
  40.6 50.3 all-gather.10
  92.7 146.3 all-gather.6
  240.7 173.1 all-gather.12
  415.4 158.7 all-gather.14
where the time goes:
time: 618 us; the launch traced here: 617 us
  waiting for transfers between devices  459 us (74%)
  blocking collectives  67.1 us (11%)
  matrix products  37 us (6%)
  local copies, waits for them, and re-layouts  22.9 us (4%)
  between operations  13.4 us (2%)
  other arithmetic  11.5 us (2%)
  starting transfers between devices  6.7 us (1%)
    all_gather x2, waiting for transfers between devices, side_by_side(): out = lax.all_gather(both, axis, axis=dim, tiled=True)  252 us
    all_gather x1, waiting for transfers between devices, on_device(): down_whole = lax.all_gather(down_proj, FS, axis=1, tiled=True)  144 us
    all_gather x2, waiting for transfers between devices, stacked_from(): pieces = lax.all_gather(pieces, axes[k], axis=0, tiled=True)  59.4 us
    all_to_all x2, blocking collectives, sum_at_owner(): lax.all_to_all(pieces, axis, split_axis=0, concat_axis=0, tiled=True)  30.5 us
    all_to_all x2, blocking collectives, copy_for_each(): lax.all_to_all(jnp.broadcast_to(value[None], (devices, *value.shape)), ax...  29.9 us
  transfers between devices with their start and end apart: 6, of which 6 were waited for; matrix products, arithmetic and copies ran while one was open for 9% of the time, Pallas kernels for 0%

commit v1 on v0

--- a/solution.py
+++ b/solution.py
@@ -153,7 +153,7 @@
         shifted = jnp.where((offset >= lag)[:, None], shifted, 0.0)
         conv = conv + taps_here[KCONV - 1 - lag] * shifted
     hidden = (jax.nn.silu(conv) * up).astype(jnp.bfloat16)
-    down_whole = lax.all_gather(down_proj, FS, axis=1, tiled=True)
+    down_whole = jnp.concatenate(lax.all_gather(down_proj, FS), axis=1)
     part = hidden
     channel_part = sum_at_owner(
         jnp.dot(part, down_whole, preferred_element_type=jnp.float32).astype(jnp.bfloat16), "tp", 0

time: 618 us -> 629 us (1.018)
  waiting for transfers between devices: 459 us -> 472 us
    all_gather x2, waiting for transfers between devices: 252 us -> 270 us  [side_by_side(): out = lax.all_gather(both, axis, axis=dim, tiled=True)]
  transfers between devices with their start and end apart: 6 -> 6, of which waited for: 6 -> 6; matrix products, arithmetic and copies ran while one was open for 9% -> 8% of each run, Pallas kernels for 0% -> 0%
where the time goes in v1:
time: 629 us
  waiting for transfers between devices  472 us (75%)
  blocking collectives  65.8 us (10%)
  matrix products  32.1 us (5%)
  local copies, waits for them, and re-layouts  28.1 us (4%)
  between operations  13.5 us (2%)
  other arithmetic  11 us (2%)
  starting transfers between devices  6.7 us (1%)
    all_gather x2, waiting for transfers between devices, side_by_side(): out = lax.all_gather(both, axis, axis=dim, tiled=True)  270 us
    all_gather x1, waiting for transfers between devices, on_device(): down_whole = jnp.concatenate(lax.all_gather(down_proj, FS), axis=1)  138 us
    all_gather x2, waiting for transfers between devices, stacked_from(): pieces = lax.all_gather(pieces, axes[k], axis=0, tiled=True)  60.4 us
    all_to_all x2, blocking collectives, copy_for_each(): lax.all_to_all(jnp.broadcast_to(value[None], (devices, *value.shape)), ax...  29.9 us
    all_to_all x2, blocking collectives, sum_at_owner(): lax.all_to_all(pieces, axis, split_axis=0, concat_axis=0, tiled=True)  29.3 us
  transfers between devices with their start and end apart: 6, of which 6 were waited for; matrix products, arithmetic and copies ran while one was open for 8% of the time, Pallas kernels for 0%

profile of v1, /device:TPU:1, one launch (start us, length us, event | category | flops | bytes accessed | tf_op | source)
XLA Modules:
  0.0 628.8 jit_solution(7844085657244020296)
XLA Ops:
  6.6 6.7 %all-gather = bf16[2048,64]{0,1:T(8,128)(2,1)S(1)} all-gather(bf16[1024,64]{0,1:T(8,128)(2,1)} %param.22), channel_id=2, replica_groups=mesh['rep'=2,'fs_0'=2,'fs_1'=4,'fs_2'=4,'tp'=2] {'fs_0'}, dimensions={0}, use_global_device_ids=true | all-gather | bytes 393216 | tf_op jit(solution)/shard_map/all_gather | solution.py:56
  13.3 0.7 copy.80
  14.1 24.9 %all-gather.10.cloned.1.call-done = bf16[8,1024,64]{1,2,0:T(8,128)(2,1)} async-done(((bf16[2,1024,64]{1,2,0:T(8,128)(2,1)}), bf16[8,1024,64]{1,2,0:T(8,128)(2,1)}) %all-gather.10.cloned.1.call-update) | async-done | bytes 1048592 | tf_op jit(solution)/shard_map/all_gather | solution.py:56
  39.1 0.7 all-gather.16.cloned.1.call-update
  39.8 0.7 pad_maximum_fusion.1
  40.6 0.8 pad_maximum_fusion
  41.4 1.6 broadcast_in_dim.32
  43.0 6.5 %all-to-all-start = ((bf16[2,256,2048]{2,1,0:T(8,128)(2,1)}), bf16[2,256,2048]{2,1,0:T(8,128)(2,1)S(1)}, u32[]{:S(2)}, u32[]{:S(2)}) async-start(bf16[2,256,2048]{2,1,0:T(8,128)(2,1)} %broadcast_in_dim.32), calls=%async_computation | async-start | bytes 4194304 | tf_op jit(solution)/shard_map/all_to_all | solution.py:25
  49.5 2.5 all-to-all-done
  52.0 0.5 multiply_reduce_fusion.1
  52.5 1.0 dynamic-slice_reduce_fusion.2
  53.6 0.1 broadcast_compare_fusion
  53.7 1.9 fusion.11
  55.5 35.5 %all-gather.12.cloned.1.call-done = bf16[32,1024,64]{1,2,0:T(8,128)(2,1)} async-done(((bf16[8,1024,64]{1,2,0:T(8,128)(2,1)}), bf16[32,1024,64]{1,2,0:T(8,128)(2,1)}) %all-gather.12.cloned.1.call-update) | async-done | bytes 4194320 | tf_op jit(solution)/shard_map/all_gather | solution.py:56
  91.1 5.0 copy.61
  96.0 138.0 %all-gather.16.cloned.1.call-done = bf16[45056,64]{0,1:T(8,128)(2,1)} async-done(((bf16[1408,64]{0,1:T(8,128)(2,1)}), bf16[45056,64]{0,1:T(8,128)(2,1)}) %all-gather.16.cloned.1.call-update) | async-done | bytes 5767184 | tf_op jit(solution)/shard_map/all_gather | solution.py:156
  234.1 3.5 copy.74
  237.6 4.5 copy.62
  242.1 159.1 %all-gather.8.cloned.1.call-done = bf16[2048,2048]{1,0:T(8,128)(2,1)} async-done(((bf16[64,2048]{1,0:T(8,128)(2,1)}), bf16[2048,2048]{1,0:T(8,128)(2,1)}) %all-gather.8.cloned.1.call-update) | async-done | bytes 8388624 | tf_op jit(solution)/shard_map/all_gather | solution.py:37
  401.2 5.2 fusion.37
  406.3 1.0 fusion.52
  407.3 24.3 %all_to_all.26 = f32[2,1,1024]{2,1,0:T(1,128)S(1)} all-to-all(f32[2,1,1024]{2,1,0:T(1,128)S(1)} %broadcast_in_dim.33), channel_id=1, replica_groups=mesh['rep'=2,'fs_0'=2,'fs_1'=4,'fs_2'=4,'tp'=2] {'tp'}, dimensions={0} | all-to-all | bytes 16384 | tf_op jit(solution)/shard_map/all_to_all | solution.py:25
  431.8 1.0 add_convert_fusion.2
  432.8 2.3 reshape.166
  435.1 2.7 bitcast_add_fusion
  437.8 3.0 copy.66
  440.8 3.5 reshape.167
  444.3 5.4 fusion.34
  449.7 2.7 convolution_convert_fusion
  452.4 5.4 all_to_all.27
  457.7 0.4 convert_reduce_fusion.1
  458.2 0.3 add_convert_fusion.1
  458.5 0.3 broadcast_in_dim.37
  458.8 5.5 all_to_all.28
  464.3 0.5 multiply_reduce_fusion
  464.8 0.2 copy-done.10
  465.0 2.0 fusion.9
  467.0 110.8 %all-gather.14.cloned.1.call-done = bf16[2048,2816]{1,0:T(8,128)(2,1)} async-done(((bf16[64,2816]{1,0:T(8,128)(2,1)}), bf16[2048,2816]{1,0:T(8,128)(2,1)}) %all-gather.14.cloned.1.call-update) | async-done | bytes 11534352 | tf_op jit(solution)/shard_map/all_gather | solution.py:37
  577.8 6.8 %fusion.12 = bf16[512,1408]{1,0:T(8,128)(2,1)S(1)} fusion(bf16[512,2048]{1,0:T(8,128)(2,1)} %fusion.9, bf16[2048,2816]{1,0:T(8,128)(2,1)} %all-gather.14.cloned.1.call-done), kind=kOutput, calls=%fused_computation.27 | convolution fusion | flops 2953510912 | bytes 9306112 | tf_op jit(solution)/shard_map/dot_general | solution.py:144
  584.6 0.2 slice.28
  584.8 0.2 slice.29
  585.1 1.1 copy-done.4
  586.2 0.9 slice-done.4
  587.1 3.4 fusion.15
  590.6 5.9 convolution_convert_fusion.1
  596.5 23.9 %all_to_all.29 = bf16[2,256,2048]{2,1,0:T(8,128)(2,1)S(1)} all-to-all(bf16[2,256,2048]{2,1,0:T(8,128)(2,1)S(1)} %bitcast.63), channel_id=1, replica_groups=mesh['rep'=2,'fs_0'=2,'fs_1'=4,'fs_2'=4,'tp'=2] {'tp'}, dimensions={0} | all-to-all | bytes 4194304 | tf_op jit(solution)/shard_map/all_to_all | solution.py:74
  620.5 0.4 convert_reduce_fusion
  620.9 1.3 add_convert_fusion
  (55 shorter events, 0.4 us)
Async XLA Ops:
  6.5 47.0 %copy-start = (f32[32,128]{1,0:T(8,128)S(1)}, f32[32,128]{1,0:T(8,128)}, u32[]{:S(2)}) copy-start(f32[32,128]{1,0:T(8,128)} %param.21) | copy-start | bytes 49156
  6.5 33.3 %copy-start.8 = (bf16[64,1024]{1,0:T(8,128)(2,1)S(1)}, bf16[64,1024]{1,0:T(8,128)(2,1)}, u32[]{:S(2)}) copy-start(bf16[64,1024]{1,0:T(8,128)(2,1)} %param.16) | copy-start | bytes 393220
  6.5 33.3 %copy-start.7 = (bf16[64,1024]{1,0:T(8,128)(2,1)S(1)}, bf16[64,1024]{1,0:T(8,128)(2,1)}, u32[]{:S(2)}) copy-start(bf16[64,1024]{1,0:T(8,128)(2,1)} %param.17) | copy-start | bytes 393220
  6.5 34.1 %copy-start.6 = (bf16[64,1408]{1,0:T(8,128)(2,1)S(1)}, bf16[64,1408]{1,0:T(8,128)(2,1)}, u32[]{:S(2)}) copy-start(bf16[64,1408]{1,0:T(8,128)(2,1)} %param.24) | copy-start | bytes 540676
  6.5 34.1 %copy-start.5 = (bf16[64,1408]{1,0:T(8,128)(2,1)S(1)}, bf16[64,1408]{1,0:T(8,128)(2,1)}, u32[]{:S(2)}) copy-start(bf16[64,1408]{1,0:T(8,128)(2,1)} %param.25) | copy-start | bytes 540676
  6.5 34.9 %copy-start.3 = (bf16[256,2048]{1,0:T(8,128)(2,1)S(1)}, bf16[256,2048]{1,0:T(8,128)(2,1)}, u32[]{:S(2)}) copy-start(bf16[256,2048]{1,0:T(8,128)(2,1)} %param.14) | copy-start | bytes 3145732
  6.6 32.4 %all-gather.10.cloned.1.call-start = ((), (), s32[]{:S(2)}) async-start(), calls=%async_computation.6 | async-start | bytes 1310720 | tf_op jit(solution)/shard_map/all_gather | solution.py:56
  14.1 77.0 %all-gather.12.cloned.1.call-start = ((), (), s32[]{:S(2)}) async-start(), calls=%async_computation.7 | async-start | bytes 5242880 | tf_op jit(solution)/shard_map/all_gather | solution.py:56
  39.0 195.0 %all-gather.16.cloned.1.call-start = ((), (), s32[]{:S(2)}) async-start(), calls=%async_computation.9 | async-start | bytes 5947392 | tf_op jit(solution)/shard_map/all_gather | solution.py:156
  39.7 361.4 %all-gather.8.cloned.1.call-start = ((), (), s32[]{:S(2)}) async-start(), calls=%async_computation.5 | async-start | bytes 8650752 | tf_op jit(solution)/shard_map/all_gather | solution.py:37
  40.6 537.2 %all-gather.14.cloned.1.call-start = ((), (), s32[]{:S(2)}) async-start(), calls=%async_computation.8 | async-start | bytes 11894784 | tf_op jit(solution)/shard_map/all_gather | solution.py:37
  43.0 9.0 %all-to-all-start = ((bf16[2,256,2048]{2,1,0:T(8,128)(2,1)}), bf16[2,256,2048]{2,1,0:T(8,128)(2,1)S(1)}, u32[]{:S(2)}, u32[]{:S(2)}) async-start(bf16[2,256,2048]{2,1,0:T(8,128)(2,1)} %broadcast_in_dim.32), calls=%async_computation | async-start | bytes 4194304 | tf_op jit(solution)/shard_map/all_to_all | solution.py:25
  49.5 4.1 copy-start.9
  242.1 189.7 %dynamic-slice-start = ((f32[2048]{0:T(1024)}, s32[]{:T(128)}), f32[1024]{0:T(1024)S(1)}, s32[]{:S(2)}) async-start(f32[2048]{0:T(1024)} %param.18, s32[]{:T(128)} %select_n.51), calls=%async_computation.12 | async-start | bytes 8704 | tf_op jit(solution)/shard_map/dynamic_slice | solution.py:121
  242.1 189.7 %dynamic-slice-start.1 = ((f32[2048]{0:T(1024)}, s32[]{:T(128)}), f32[1024]{0:T(1024)S(1)}, s32[]{:S(2)}) async-start(f32[2048]{0:T(1024)} %param.19, s32[]{:T(128)} %select_n.51), calls=%async_computation.13 | async-start | bytes 8704 | tf_op jit(solution)/shard_map/dynamic_slice | solution.py:122
  444.3 5.4 copy-start.2
  464.3 0.7 copy-start.10
  577.8 7.3 %slice-start.2 = ((s8[11534336]{0:T(1024)(128)(4,1)}), s8[4194304]{0:T(1024)(128)(4,1)S(1)}, s32[]{:S(2)}) async-start(s8[11534336]{0:T(1024)(128)(4,1)} %bitcast.69), calls=%async_computation.14 | async-start | bytes 8388608
  577.8 7.3 %slice-start.3 = ((s8[11534336]{0:T(1024)(128)(4,1)}), s8[4194304]{0:T(1024)(128)(4,1)S(1)}, s32[]{:S(2)}) async-start(s8[11534336]{0:T(1024)(128)(4,1)} %bitcast.69), calls=%async_computation.15 | async-start | bytes 8388608
  584.6 1.6 copy-start.4
  584.6 2.5 slice-start.4
  584.8 5.7 slice-start
  587.1 3.4 slice-start.1
  620.5 1.8 copy-start.1
Sparse Core Ops, SparseCore 0:
  14.2 24.7 all-gather.9
  40.6 50.3 all-gather.11
  92.8 141.2 all-gather.15
  235.6 165.5 all-gather.7
  402.7 175.0 all-gather.13
